TPU v7x, 32 devices: a whole 2x2x4 slice. The times are simulated.
32 devices in a mesh: rep: 2 (over x), fs: 8 (over z, y), tp: 2 (over core).
Axes of the slice: x: 2, y: 2, z: 4, core: 2. Of those that a mesh axis runs over, the one named last changes fastest.
Arguments:
- resid: bfloat16 [12288, 2048], P(('rep', 'fs', 'tp')), may hold values from -6 to 6
- mix_gain: float32 [2048], replicated, may hold values from 0.1 to 1.9
- query_weight: bfloat16 [2048, 1024], P('fs', 'tp'), may hold values from -0.125 to 0.125
- key_weight: bfloat16 [2048, 1024], P('fs', 'tp'), may hold values from -0.125 to 0.125
- value_weight: bfloat16 [2048, 2048], P('fs', 'tp'), may hold values from -0.125 to 0.125
- head_gain: float32 [2048], P('tp'), may hold values from 0.1 to 1.9
- out_weight: bfloat16 [2048, 2048], P('tp', 'fs'), may hold values from -0.125 to 0.125
- mlp_gain: float32 [2048], replicated, may hold values from 0.1 to 1.9
- gate_weight: bfloat16 [2048, 2816], P('fs', 'tp'), may hold values from -0.125 to 0.125
- up_weight: bfloat16 [2048, 2816], P('fs', 'tp'), may hold values from -0.125 to 0.125
- down_weight: bfloat16 [2816, 2048], P('tp', 'fs'), may hold values from -0.109375 to 0.109375
Outputs:
- layer_out: bfloat16 [12288, 2048], P(('rep', 'fs', 'tp'))
All inputs are finite; a program needn't handle non-finite values.
Results may differ from a plain program's by a relative error of at most 0.014.
Values may be sent and summed in bfloat16 or wider, within the bound.
A program may use at most 128 MiB of HBM per device.

v0:
```python
import jax
import jax.numpy as jnp
from jax import lax
from jax.sharding import PartitionSpec as P

DK = 256
DV = 512
BLOCK = 128


norm_eps = 1e-06
rope_base = 10000.0


def rms_scale(values, gain):
    widened = values.astype(jnp.float32)
    scaled = widened * lax.rsqrt(jnp.mean(widened * widened, axis=-1, keepdims=True) + norm_eps)
    return (scaled * gain).astype(jnp.bfloat16)


def rotate(vectors):
    length_total = vectors.shape[0]
    half_width = vectors.shape[-1] // 2
    position = jnp.arange(length_total, dtype=jnp.float32)
    inverse = 1.0 / rope_base ** jnp.linspace(0.0, 1.0, half_width, dtype=jnp.float32)
    angle = position[:, None] * inverse[None, :]
    cosine = jnp.cos(angle)[:, None, :]
    sine = jnp.sin(angle)[:, None, :]
    first = vectors[..., :half_width]
    second = vectors[..., half_width:]
    return jnp.concatenate(
        [first * cosine - second * sine, second * cosine + first * sine], axis=-1
    )


def decay_tables(head_ids, block):
    log_gamma = jnp.log1p(-(2.0 ** (-5.0 - 2.0 * head_ids.astype(jnp.float32))))
    offset = jnp.arange(block, dtype=jnp.float32)
    distance = offset[:, None] - offset[None, :]
    inside = jnp.where(
        distance >= 0, jnp.exp(log_gamma[:, None, None] * jnp.maximum(distance, 0.0)), 0.0
    )
    query_decay = jnp.exp(log_gamma[:, None] * (offset + 1.0))
    key_decay = jnp.exp(log_gamma[:, None] * (block - 1.0 - offset))
    block_decay = jnp.exp(log_gamma * block)
    return (inside, query_decay, key_decay, block_decay)


def retain(queries, keys, values, head_ids, block):
    length_total, heads, key_width = queries.shape
    value_width = values.shape[-1]
    count = length_total // block
    inside, query_decay, key_decay, block_decay = decay_tables(head_ids, block)

    def blocks(tensor):
        return tensor.reshape(count, block, heads, tensor.shape[-1]).transpose(0, 2, 1, 3)

    def advance(memory, inputs):
        query_tile_rows, key_tile_rows, value_block = inputs
        attention_scores = jnp.einsum(
            "zvf,zjf->zvj", query_tile_rows, key_tile_rows, preferred_element_type=jnp.float32
        )
        weights = (attention_scores * inside).astype(jnp.bfloat16)
        within = jnp.einsum(
            "hlm,hmv->hlv", weights, value_block, preferred_element_type=jnp.float32
        )
        carried = (
            jnp.einsum(
                "hld,hdv->hlv",
                query_tile_rows,
                memory.astype(jnp.bfloat16),
                preferred_element_type=jnp.float32,
            )
            * query_decay[:, :, None]
        )
        weighted_keys = (key_tile_rows.astype(jnp.float32) * key_decay[:, :, None]).astype(
            jnp.bfloat16
        )
        memory = memory * block_decay[:, None, None] + jnp.einsum(
            "hld,hlv->hdv", weighted_keys, value_block, preferred_element_type=jnp.float32
        )
        return (memory, within + carried)

    start_state = jnp.zeros((heads, key_width, value_width), jnp.float32)
    _, outputs = lax.scan(advance, start_state, (blocks(queries), blocks(keys), blocks(values)))
    return outputs.transpose(0, 2, 1, 3).reshape(length_total, heads, value_width)


def head_scale(retained, gain):
    scaled = retained * lax.rsqrt(jnp.mean(retained * retained, axis=-1, keepdims=True) + norm_eps)
    return (scaled.reshape(retained.shape[0], -1) * gain).astype(jnp.bfloat16)


def shards(
    resid,
    mix_gain,
    query_weight,
    key_weight,
    value_weight,
    head_gain,
    out_weight,
    mlp_gain,
    gate_weight,
    up_weight,
    down_weight,
):
    token_rows = resid.shape[0]
    length_total = token_rows * lax.axis_size("tp")
    key_cols = query_weight.shape[1]
    heads_here = key_cols // DK
    normed = rms_scale(resid, mix_gain)
    mixer_shard = jnp.concatenate([query_weight, key_weight, value_weight], axis=1)
    mixer_full = lax.all_gather(mixer_shard, "fs", axis=0, tiled=True)
    projected = jnp.dot(
        lax.all_gather(normed, "tp", axis=0, tiled=True),
        mixer_full,
        preferred_element_type=jnp.float32,
    ).astype(jnp.bfloat16)
    queries = projected[:, :key_cols].astype(jnp.float32).reshape(length_total, heads_here, DK)
    keys = (
        projected[:, key_cols : 2 * key_cols]
        .astype(jnp.float32)
        .reshape(length_total, heads_here, DK)
    )
    values = projected[:, 2 * key_cols :].reshape(length_total, heads_here, DV)
    query_rot = rotate(queries).astype(jnp.bfloat16)
    key_rot = (rotate(keys) * DK ** (-0.5)).astype(jnp.bfloat16)
    head_ids = lax.axis_index("tp") * heads_here + jnp.arange(heads_here, dtype=jnp.int32)
    retained = retain(query_rot, key_rot, values, head_ids, BLOCK)
    head_out = head_scale(retained, head_gain)
    out_full = lax.all_gather(out_weight, "fs", axis=1, tiled=True)
    selected = head_out
    mixer_sum = lax.psum_scatter(
        jnp.dot(selected, out_full, preferred_element_type=jnp.float32).astype(jnp.bfloat16),
        "tp",
        scatter_dimension=0,
        tiled=True,
    ).astype(jnp.float32)
    middle = (resid.astype(jnp.float32) + mixer_sum).astype(jnp.bfloat16)
    normed_mlp = rms_scale(middle, mlp_gain)
    local_units = gate_weight.shape[1]
    mlp_shard = jnp.concatenate([gate_weight, up_weight], axis=1)
    mlp_full = lax.all_gather(mlp_shard, "fs", axis=0, tiled=True)
    both = jnp.dot(
        lax.all_gather(normed_mlp, "tp", axis=0, tiled=True),
        mlp_full,
        preferred_element_type=jnp.float32,
    )
    hidden_units = (jax.nn.silu(both[:, :local_units]) * both[:, local_units:]).astype(jnp.bfloat16)
    down_full = lax.all_gather(down_weight, "fs", axis=1, tiled=True)
    selected = hidden_units
    mlp_sum = lax.psum_scatter(
        jnp.dot(selected, down_full, preferred_element_type=jnp.float32).astype(jnp.bfloat16),
        "tp",
        scatter_dimension=0,
        tiled=True,
    ).astype(jnp.float32)
    return (middle.astype(jnp.float32) + mlp_sum).astype(jnp.bfloat16)


def solution(mesh):
    placed = (
        P(("rep", "fs", "tp"), None),
        P(),
        P("fs", "tp"),
        P("fs", "tp"),
        P("fs", "tp"),
        P("tp"),
        P("tp", "fs"),
        P(),
        P("fs", "tp"),
        P("fs", "tp"),
        P("tp", "fs"),
    )
    return jax.shard_map(
        shards, mesh=mesh, in_specs=placed, out_specs=P(("rep", "fs", "tp"), None), check_vma=False
    )
```

profile of v0, /device:TPU:0, one launch (start us, length us, event | category | flops | bytes accessed | tf_op | source)
XLA Modules:
  0.0 551.8 jit_solution(12479587014946529048)
XLA Ops:
  6.5 1.9 fusion.44
  8.4 3.0 fusion.46
  11.5 1.1 pad_maximum_fusion.1
  12.7 0.7 all-gather.11.cloned.1.call-update
  13.6 0.1 fusion.61
  13.6 2.3 fusion.58
  15.9 10.5 %all-gather.7.cloned.1.call-done = bf16[768,2048]{1,0:T(8,128)(2,1)} async-done(((bf16[384,2048]{1,0:T(8,128)(2,1)}), bf16[768,2048]{1,0:T(8,128)(2,1)}) %all-gather.7.cloned.1.call-update) | async-done | bytes 3145744 | tf_op jit(solution)/shard_map/all_gather | solution.py:115
  26.4 127.8 %all-gather.9.cloned.1.call-done = bf16[2048,2048]{1,0:T(8,128)(2,1)} async-done(((bf16[256,2048]{1,0:T(8,128)(2,1)}), bf16[2048,2048]{1,0:T(8,128)(2,1)}) %all-gather.9.cloned.1.call-update) | async-done | bytes 8388624 | tf_op jit(solution)/shard_map/all_gather | solution.py:113
  154.2 10.0 %convolution_convert_fusion = bf16[768,2048]{1,0:T(8,128)(2,1)S(1)} fusion(bf16[768,2048]{1,0:T(8,128)(2,1)} %all-gather.7.cloned.1.call-done, bf16[2048,2048]{1,0:T(8,128)(2,1)} %all-gather.9.cloned.1.call-done), kind=kOutput, calls=%fused_computation.51 | convolution fusion | flops 6444023808 | bytes 14680064 | tf_op jit(solution)/shard_map/dot_general | solution.py:114
  164.3 2.4 slice_convert_fusion
  166.7 0.2 copy-done.3
  167.0 3.2 reshape.150
  170.1 3.1 reshape.152
  173.2 2.3 reshape_reshape.3
  175.6 1.8 copy.58
  177.5 0.5 copy-done.5
  177.9 1.1 fusion.63
  179.1 0.4 subtract_convert_fusion
  179.5 1.0 maximum_bitcast_fusion
  180.5 1.0 fusion.56
  181.5 28.8 %while.15 = (s32[]{:T(128)}, f32[2,256,512]{2,1,0:T(8,128)S(1)}, f32[6,2,128,512]{3,2,1,0:T(8,128)}, bf16[6,2,128,256]{3,2,0,1:T(8,128)(2,1)}, bf16[6,2,128,512]...) while((s32[]{:T(128)}, f32[2,256,512]{2,1,0:T(8,128)S(1)}, ...), condition=%wide.region_2.4_spmd.clone.clone.clone, body=%wide.region_1.3_spmd.clone.clone.clone.sunk | while | flops 186188304 | bytes 5858980 | solution.py:85
  181.6 1.1 convolution_multiply_fusion.3
  182.7 2.2 fusion.83
  184.9 1.4 convolution_add_fusion.3
  186.3 0.1 multiply_exponential_fusion.6
  186.4 1.1 convolution_multiply_fusion.3
  187.6 2.1 fusion.83
  189.7 1.4 convolution_add_fusion.3
  191.2 1.2 convolution_multiply_fusion.3
  192.3 2.1 fusion.83
  194.5 1.4 convolution_add_fusion.3
  196.0 1.1 convolution_multiply_fusion.3
  197.1 2.2 fusion.83
  199.3 1.4 convolution_add_fusion.3
  200.8 1.1 convolution_multiply_fusion.3
  202.0 2.2 fusion.83
  204.1 1.4 convolution_add_fusion.3
  205.5 0.1 multiply_exponential_fusion.6
  205.6 1.1 convolution_multiply_fusion.3
  206.8 2.1 fusion.83
  208.9 1.4 convolution_add_fusion.3
  210.3 2.2 multiply_reduce_fusion
  212.5 0.2 copy.39
  212.7 1.2 mul.286
  214.0 0.8 copy.48
  214.7 1.1 copy-done.2
  215.9 2.4 copy.38
  218.3 2.4 copy.47
  220.7 8.4 %all-gather.11.cloned.1.call-done = bf16[1024,2048]{1,0:T(8,128)(2,1)} async-done(((bf16[1024,256]{1,0:T(8,128)(2,1)}), bf16[1024,2048]{1,0:T(8,128)(2,1)}) %all-gather.11.cloned.1.call-update) | async-done | bytes 4194320 | tf_op jit(solution)/shard_map/all_gather | solution.py:131
  229.1 8.2 %convolution_convert_fusion.1 = bf16[768,2048]{1,0:T(8,128)(2,1)} fusion(bf16[1024,2048]{1,0:T(8,128)(2,1)} %all-gather.11.cloned.1.call-done, f32[768,1024]{1,0:T(8,128)} %bitcast.73, f32[768,1024]{1,0:T(8,128)S(1)} %bitcast.72, f32[1024]{0:T(1024)S(1)} %copy-done.14), kind=kOutput, calls=%fused_computation.52 | convolution fusion | flops 3225157632 | bytes 13635584 | tf_op jit(solution)/shard_map/dot_general | solution.py:134
  237.4 1.0 copy-done.8
  238.4 0.2 copy-done.9
  238.6 1.2 pad_maximum_fusion
  239.9 6.9 %reduce-scatter.3.cloned.1.call-done = bf16[384,2048]{1,0:T(8,128)(2,1)} async-done(((bf16[768,2048]{1,0:T(8,128)(2,1)}), bf16[384,2048]{1,0:T(8,128)(2,1)}) %reduce-scatter.3.cloned.1.call-update) | async-done | bytes 1572880 | tf_op jit(solution)/shard_map/reduce_scatter | solution.py:133
  246.9 2.1 fusion.48
  249.0 1.9 fusion.50
  251.0 0.7 all-gather.17.cloned.1.call-update
  251.7 161.9 %all-gather.15.cloned.1.call-done = bf16[2048,2816]{1,0:T(8,128)(2,1)} async-done(((bf16[256,2816]{1,0:T(8,128)(2,1)}), bf16[2048,2816]{1,0:T(8,128)(2,1)}) %all-gather.15.cloned.1.call-update) | async-done | bytes 11534352 | tf_op jit(solution)/shard_map/all_gather | solution.py:143
  413.6 11.7 %all-gather.13.cloned.1.call-done = bf16[768,2048]{1,0:T(8,128)(2,1)} async-done(((bf16[384,2048]{1,0:T(8,128)(2,1)}), bf16[768,2048]{1,0:T(8,128)(2,1)}) %all-gather.13.cloned.1.call-update) | async-done | bytes 3145744 | tf_op jit(solution)/shard_map/all_gather | solution.py:145
  425.3 15.7 %fusion.65 = f32[768,2816]{1,0:T(8,128)} fusion(bf16[768,2048]{1,0:T(8,128)(2,1)} %all-gather.13.cloned.1.call-done, bf16[2048,2816]{1,0:T(8,128)(2,1)} %all-gather.15.cloned.1.call-done), kind=kOutput, calls=%fused_computation.97 | convolution fusion | flops 8858370048 | bytes 23330816 | tf_op jit(solution)/shard_map/dot_general | solution.py:144
  441.0 80.7 %all-gather.17.cloned.1.call-done = bf16[1408,2048]{1,0:T(8,128)(2,1)} async-done(((bf16[1408,256]{1,0:T(8,128)(2,1)}), bf16[1408,2048]{1,0:T(8,128)(2,1)}) %all-gather.17.cloned.1.call-update) | async-done | bytes 5767184 | tf_op jit(solution)/shard_map/all_gather | solution.py:150
  521.7 10.4 %convolution_convert_fusion.2 = bf16[768,2048]{1,0:T(8,128)(2,1)} fusion(bf16[1408,2048]{1,0:T(8,128)(2,1)} %all-gather.17.cloned.1.call-done, f32[768,2816]{1,0:T(8,128)} %fusion.65), kind=kOutput, calls=%fused_computation.53 | convolution fusion | flops 4437245952 | bytes 17563648 | tf_op jit(solution)/shard_map/dot_general | solution.py:153
  532.1 9.5 %reduce-scatter.5.cloned.1.call-done = bf16[384,2048]{1,0:T(8,128)(2,1)} async-done(((bf16[768,2048]{1,0:T(8,128)(2,1)}), bf16[384,2048]{1,0:T(8,128)(2,1)}) %reduce-scatter.5.cloned.1.call-update) | async-done | bytes 1572880 | tf_op jit(solution)/shard_map/reduce_scatter | solution.py:152
  541.6 3.4 fusion.51
  (61 shorter events, 1.0 us)
Async XLA Ops:
  6.5 19.9 %all-gather.7.cloned.1.call-start = ((), (), s32[]{:S(2)}) async-start(), calls=%async_computation.2 | async-start | bytes 4718592 | tf_op jit(solution)/shard_map/all_gather | solution.py:115
  6.5 5.0 copy-start.10
  6.5 5.0 copy-start.11
  6.5 5.0 copy-start.12
  11.4 142.8 %all-gather.9.cloned.1.call-start = ((), (), s32[]{:S(2)}) async-start(), calls=%async_computation.3 | async-start | bytes 9437184 | tf_op jit(solution)/shard_map/all_gather | solution.py:113
  12.7 216.4 %all-gather.11.cloned.1.call-start = ((), (), s32[]{:S(2)}) async-start(), calls=%async_computation.4 | async-start | bytes 4718592 | tf_op jit(solution)/shard_map/all_gather | solution.py:131
  13.4 233.5 %reduce-scatter.3.cloned.1.call-start = ((), (), s32[]{:S(2)}) async-start(), calls=%async_computation.5 | async-start | bytes 4718592 | tf_op jit(solution)/shard_map/reduce_scatter | solution.py:133
  164.3 2.7 copy-start.3
  167.0 6.3 %slice-start = ((bf16[768,2048]{1,0:T(8,128)(2,1)}), bf16[768,1024]{1,0:T(8,128)(2,1)S(1)}, s32[]{:S(2)}) async-start(bf16[768,2048]{1,0:T(8,128)(2,1)} %copy-done.3), calls=%async_computation.10 | async-start | bytes 3145728 | tf_op jit(solution)/shard_map/slice | solution.py:125
  175.6 1.9 copy-start.4
  175.6 2.4 copy-start.5
  177.9 1.1 copy-start.6
  177.9 1.1 copy-start.7
  214.0 1.9 copy-start.2
  218.3 10.8 %copy-start.14 = (f32[1024]{0:T(1024)S(1)}, f32[1024]{0:T(1024)}, u32[]{:S(2)}) copy-start(f32[1024]{0:T(1024)} %param.20) | copy-start | bytes 12292
  237.3 1.1 copy-start.8
  237.3 1.3 copy-start.9
  237.3 9.6 %copy-start = (bf16[384,2048]{1,0:T(8,128)(2,1)S(1)}, bf16[384,2048]{1,0:T(8,128)(2,1)}, u32[]{:S(2)}) copy-start(bf16[384,2048]{1,0:T(8,128)(2,1)} %param.15) | copy-start | bytes 4718596
  237.3 11.7 %copy-start.13 = (f32[2048]{0:T(1024)S(1)}, f32[2048]{0:T(1024)}, u32[]{:S(2)}) copy-start(f32[2048]{0:T(1024)} %param.22) | copy-start | bytes 24580
  237.3 176.2 %all-gather.15.cloned.1.call-start = ((), (), s32[]{:S(2)}) async-start(), calls=%async_computation.7 | async-start | bytes 12976128 | tf_op jit(solution)/shard_map/all_gather | solution.py:143
  239.9 185.4 %all-gather.13.cloned.1.call-start = ((), (), s32[]{:S(2)}) async-start(), calls=%async_computation.6 | async-start | bytes 4718592 | tf_op jit(solution)/shard_map/all_gather | solution.py:145
  246.9 2.1 copy-start.1
  250.9 270.8 %all-gather.17.cloned.1.call-start = ((), (), s32[]{:S(2)}) async-start(), calls=%async_computation.8 | async-start | bytes 6488064 | tf_op jit(solution)/shard_map/all_gather | solution.py:150
  251.7 289.9 %reduce-scatter.5.cloned.1.call-start = ((), (), s32[]{:S(2)}) async-start(), calls=%async_computation.9 | async-start | bytes 4718592 | tf_op jit(solution)/shard_map/reduce_scatter | solution.py:152
Sparse Core Ops, SparseCore 0:
  11.6 14.8 all-gather.6
  28.6 125.6 all-gather.8
  156.3 72.7 all-gather.10
  237.5 9.3 reduce-scatter.2
  248.9 164.6 all-gather.14
  415.0 10.2 all-gather.12
  427.3 94.2 all-gather.16
  532.2 9.3 reduce-scatter.4
where the time goes:
time: 552 us
  waiting for transfers between devices  419 us (76%)
  matrix products  72.4 us (13%)
  other arithmetic  24.6 us (4%)
  local copies, waits for them, and re-layouts  21.7 us (4%)
  between operations  13.7 us (2%)
    all_gather x1, waiting for transfers between devices, shards(): mlp_full = lax.all_gather(mlp_shard, 'fs', axis=0, tiled=True)  162 us
    all_gather x1, waiting for transfers between devices, shards(): mixer_full = lax.all_gather(mixer_shard, 'fs', axis=0, tiled=True)  128 us
    all_gather x1, waiting for transfers between devices, shards(): down_full = lax.all_gather(down_weight, 'fs', axis=1, tiled=True)  80.7 us
    dot_general x1, matrix products, shards(): jnp.dot(lax.all_gather(normed_mlp, 'tp', axis=0, tiled=True), mlp_full, p...  15.7 us
    dot_general x6, matrix products, advance(): jnp.einsum('hlm,hmv->hlv', weights, value_block, preferred_element_type=j...  12.8 us
    all_gather x1, waiting for transfers between devices, shards(): lax.all_gather(normed_mlp, 'tp', axis=0, tiled=True)  11.7 us
  transfers between devices with their start and end apart: 8, of which 8 were waited for; matrix products, arithmetic and copies ran while one was open for 16% of the time, Pallas kernels for 0%

commit v1 on v0

--- a/solution.py
+++ b/solution.py
@@ -1,7 +1,213 @@
+import functools
+
 import jax
 import jax.numpy as jnp
 from jax import lax
+from jax.experimental import pallas as pl
+from jax.experimental.pallas import tpu as pltpu
 from jax.sharding import PartitionSpec as P
+
+UNITS = 8
+MESH = pl.DeviceIdType.MESH
+
+
+class Exchange:
+    def __init__(self, depth, shards, fulls, axes, send_sem, recv_sem):
+        self.depth = depth
+        self.shards, self.fulls, self.axes = shards, fulls, axes
+        self.send_sem, self.recv_sem = send_sem, recv_sem
+        self.x = lax.axis_index("rep")
+        fs = lax.axis_index("fs")
+        self.z = fs // 2
+        self.y = lax.rem(fs, 2)
+
+    def barrier(self):
+        sem = pltpu.get_barrier_semaphore()
+        z, y, x = self.z, self.y, self.x
+        pl.semaphore_signal(sem, inc=1, device_id={"rep": 1 - x}, device_id_type=MESH)
+        pl.semaphore_signal(sem, inc=1, device_id={"fs": z * 2 + 1 - y}, device_id_type=MESH)
+
+        @pl.when(z > 0)
+        def _():
+            pl.semaphore_signal(sem, inc=1, device_id={"fs": (z - 1) * 2 + y}, device_id_type=MESH)
+
+        @pl.when(z < self.depth - 1)
+        def _():
+            pl.semaphore_signal(sem, inc=1, device_id={"fs": (z + 1) * 2 + y}, device_id_type=MESH)
+
+        low = jnp.minimum(z, 1)
+        high = jnp.minimum(self.depth - 1 - z, 1)
+        pl.semaphore_wait(sem, 2 + low + high)
+
+    def slot(self, w, block, start, count):
+        rows, cols = self.shards[w].shape
+        if self.axes[w] == 0:
+            first = pl.multiple_of(block * rows + start, 16)
+            return self.fulls[w].at[pl.ds(first, count), :]
+        return self.fulls[w].at[
+            pl.ds(pl.multiple_of(start, 16), count), pl.ds(pl.multiple_of(block * cols, 128), cols)
+        ]
+
+    def copy(self, w, kind, origin, own=False, incoming=False):
+        x, y, z = self.x, self.y, self.z
+        unit = self.shards[w].shape[0] // UNITS
+        xs = 1 - x if incoming and kind in ("x1", "x2") else x
+        start, count = {
+            "up": (2 * x, 6), "down": (2 * x, 6), "y": (3 * x, 5), "x1": (6 * xs, 2), "x2": (5 * xs, 3),
+        }[kind]
+        start, count = start * unit, count * unit
+        far = kind == "x2" or (incoming and kind == "y")
+        block = origin * 2 + (1 - y if far else y)
+        target = {
+            "up": {"fs": (z + 1) * 2 + y},
+            "down": {"fs": (z - 1) * 2 + y},
+            "y": {"fs": z * 2 + 1 - y},
+            "x1": {"rep": 1 - x},
+            "x2": {"rep": 1 - x},
+        }[kind]
+        place = self.slot(w, block, start, count)
+        source = place
+        if own:
+            source = self.shards[w].at[pl.ds(pl.multiple_of(start, 16), count), :]
+        sends = ("up", "down", "y", "x1", "x2").index(kind)
+        receives = (0, 0, 1, 2, 3)[sends]
+        return pltpu.make_async_remote_copy(
+            src_ref=source,
+            dst_ref=place,
+            send_sem=self.send_sem.at[w, sends, origin],
+            recv_sem=self.recv_sem.at[w, receives, origin],
+            device_id=target,
+            device_id_type=MESH,
+        )
+
+    def each(self, t, body):
+        if t == 0:
+            body("own", self.z)
+            return
+
+        @pl.when(self.z - t >= 0)
+        def _():
+            body("up", self.z - t)
+
+        @pl.when(self.z + t < self.depth)
+        def _():
+            body("down", self.z + t)
+
+    def onward(self, w, way, origin, act):
+        if way in ("own", "up"):
+
+            @pl.when(self.z < self.depth - 1)
+            def _():
+                act(self.copy(w, "up", origin, own=way == "own"))
+
+        if way in ("own", "down"):
+
+            @pl.when(self.z > 0)
+            def _():
+                act(self.copy(w, "down", origin, own=way == "own"))
+
+    def step(self, w, t):
+        if t < self.depth:
+
+            def arrive(way, origin):
+                if way != "own":
+                    self.copy(w, way, origin, incoming=True).wait_recv()
+                self.onward(w, way, origin, lambda c: c.start())
+                self.copy(w, "y", origin, own=way == "own").start()
+                if way != "own":
+                    self.copy(w, "x1", origin).start()
+
+            self.each(t, arrive)
+        if 1 <= t <= self.depth:
+
+            def cross(way, origin):
+                self.copy(w, "y", origin, incoming=True).wait_recv()
+                self.copy(w, "x2", origin).start()
+
+            self.each(t - 1, cross)
+        if t == self.depth + 1:
+            for s in range(self.depth):
+
+                def last(way, origin):
+                    if way != "own":
+                        self.copy(w, "x1", origin, incoming=True).wait_recv()
+                    self.copy(w, "x2", origin, incoming=True).wait_recv()
+
+                self.each(s, last)
+
+    def drain(self, w):
+        for s in range(self.depth):
+
+            def sent(way, origin):
+                self.onward(w, way, origin, lambda c: c.wait_send())
+                self.copy(w, "y", origin, own=way == "own").wait_send()
+                if way != "own":
+                    self.copy(w, "x1", origin).wait_send()
+                self.copy(w, "x2", origin).wait_send()
+
+            self.each(s, sent)
+
+
+def gather_kernel(depth, axes, *refs):
+    count = len(axes)
+    shards, fulls = refs[:count], refs[count : 2 * count]
+    held = refs[2 * count : 3 * count]
+    send_sem, recv_sem, load_sem, store_sem = refs[3 * count :]
+    ex = Exchange(depth, shards, fulls, axes, send_sem, recv_sem)
+    loads = [pltpu.make_async_copy(shards[w], held[w], load_sem.at[w]) for w in range(count)]
+    for copy in loads:
+        copy.start()
+    ex.barrier()
+    fs = lax.axis_index("fs")
+    stores = [
+        pltpu.make_async_copy(
+            held[w], ex.slot(w, fs, 0, shards[w].shape[0]), store_sem.at[w]
+        )
+        for w in range(count)
+    ]
+    pace = depth - 1
+    for tick in range(pace * (count - 1) + depth + 2):
+        for w in range(count):
+            t = tick - pace * w
+            if 0 <= t <= depth + 1:
+                ex.step(w, t)
+        if tick == 0:
+            for load, store in zip(loads, stores):
+                load.wait()
+                store.start()
+    for copy in stores:
+        copy.wait()
+    for w in range(count):
+        ex.drain(w)
+
+
+def gather_all(shards, axes):
+    size = lax.axis_size("fs")
+    fits = all(s.shape[0] % (UNITS * 16) == 0 and s.shape[1] % 128 == 0 for s in shards)
+    if lax.axis_size("rep") != 2 or size % 2 or not fits:
+        return [lax.all_gather(s, "fs", axis=a, tiled=True) for s, a in zip(shards, axes)]
+    depth = size // 2
+    count = len(shards)
+    shapes = []
+    for s, a in zip(shards, axes):
+        shape = list(s.shape)
+        shape[a] *= size
+        shapes.append(jax.ShapeDtypeStruct(tuple(shape), s.dtype))
+    return pl.pallas_call(
+        functools.partial(gather_kernel, depth, tuple(axes)),
+        out_shape=shapes,
+        in_specs=[pl.BlockSpec(memory_space=pl.ANY)] * count,
+        out_specs=[pl.BlockSpec(memory_space=pl.ANY)] * count,
+        scratch_shapes=[pltpu.VMEM(s.shape, s.dtype) for s in shards]
+        + [
+            pltpu.SemaphoreType.DMA((count, 5, depth)),
+            pltpu.SemaphoreType.DMA((count, 4, depth)),
+            pltpu.SemaphoreType.DMA((count,)),
+            pltpu.SemaphoreType.DMA((count,)),
+        ],
+        compiler_params=pltpu.CompilerParams(collective_id=0, has_side_effects=True),
+    )(*shards)
+
 
 DK = 256
 DV = 512
@@ -110,7 +316,10 @@
     heads_here = key_cols // DK
     normed = rms_scale(resid, mix_gain)
     mixer_shard = jnp.concatenate([query_weight, key_weight, value_weight], axis=1)
-    mixer_full = lax.all_gather(mixer_shard, "fs", axis=0, tiled=True)
+    mlp_shard = jnp.concatenate([gate_weight, up_weight], axis=1)
+    mixer_full, out_full, mlp_full, down_full = gather_all(
+        [mixer_shard, out_weight, mlp_shard, down_weight], [0, 1, 0, 1]
+    )
     projected = jnp.dot(
         lax.all_gather(normed, "tp", axis=0, tiled=True),
         mixer_full,
@@ -128,7 +337,6 @@
     head_ids = lax.axis_index("tp") * heads_here + jnp.arange(heads_here, dtype=jnp.int32)
     retained = retain(query_rot, key_rot, values, head_ids, BLOCK)
     head_out = head_scale(retained, head_gain)
-    out_full = lax.all_gather(out_weight, "fs", axis=1, tiled=True)
     selected = head_out
     mixer_sum = lax.psum_scatter(
         jnp.dot(selected, out_full, preferred_element_type=jnp.float32).astype(jnp.bfloat16),
@@ -139,15 +347,12 @@
     middle = (resid.astype(jnp.float32) + mixer_sum).astype(jnp.bfloat16)
     normed_mlp = rms_scale(middle, mlp_gain)
     local_units = gate_weight.shape[1]
-    mlp_shard = jnp.concatenate([gate_weight, up_weight], axis=1)
-    mlp_full = lax.all_gather(mlp_shard, "fs", axis=0, tiled=True)
     both = jnp.dot(
         lax.all_gather(normed_mlp, "tp", axis=0, tiled=True),
         mlp_full,
         preferred_element_type=jnp.float32,
     )
     hidden_units = (jax.nn.silu(both[:, :local_units]) * both[:, local_units:]).astype(jnp.bfloat16)
-    down_full = lax.all_gather(down_weight, "fs", axis=1, tiled=True)
     selected = hidden_units
     mlp_sum = lax.psum_scatter(
         jnp.dot(selected, down_full, preferred_element_type=jnp.float32).astype(jnp.bfloat16),

time: 552 us -> 390 us (0.71)
  waiting for transfers between devices: 419 us -> 34.2 us
  Pallas kernels: 0 us -> 230 us
  matrix products: 72.4 us -> 65.7 us
    all_gather x4 -> x0, waiting for transfers between devices: 379 us -> none  [the longest x1 162 us: shards(): mlp_full = lax.all_gather(mlp_shard, 'fs', axis=0, tiled=True)]
    pallas_call x0 -> x1, Pallas kernels: none -> 230 us  [gather_all(): pl.pallas_call(functools.partial(gather_kernel, depth, tuple(axes)), out_...]
    all_gather x1, waiting for transfers between devices: 10.5 us -> 0.01 us  [shards(): lax.all_gather(normed, 'tp', axis=0, tiled=True)]
  transfers between devices with their start and end apart: 8 -> 4, of which waited for: 8 -> 3; matrix products, arithmetic and copies ran while one was open for 16% -> 1% of each run, Pallas kernels for 0% -> 59%
where the time goes in v1:
time: 390 us; the launch traced here: 389 us
  Pallas kernels  230 us (59%)
  matrix products  65.7 us (17%)
  waiting for transfers between devices  34.2 us (9%)
  other arithmetic  24.8 us (6%)
  local copies, waits for them, and re-layouts  20.2 us (5%)
  between operations  13.4 us (3%)
    pallas_call x1, Pallas kernels, gather_all(): pl.pallas_call(functools.partial(gather_kernel, depth, tuple(axes)), out_...  230 us
    dot_general x1, matrix products, shards(): jnp.dot(lax.all_gather(normed_mlp, 'tp', axis=0, tiled=True), mlp_full, p...  13.7 us
    all_gather x1, waiting for transfers between devices, shards(): lax.all_gather(normed_mlp, 'tp', axis=0, tiled=True)  13.5 us
    dot_general x6, matrix products, advance(): jnp.einsum('hlm,hmv->hlv', weights, value_block, preferred_element_type=j...  12.8 us
    reduce_scatter x1, waiting for transfers between devices, shards(): lax.psum_scatter(jnp.dot(selected, down_full, preferred_element_type=jnp....  12.5 us
    dot_general x1, matrix products, shards(): jnp.dot(lax.all_gather(normed, 'tp', axis=0, tiled=True), mixer_full, pre...  10 us
    dot_general x1, matrix products, shards(): jnp.dot(selected, down_full, preferred_element_type=jnp.float32)  9.17 us
    dot_general x6, matrix products, advance(): jnp.einsum('hld,hlv->hdv', weighted_keys, value_block, preferred_element_...  8.39 us
  transfers between devices with their start and end apart: 4, of which 3 were waited for; matrix products, arithmetic and copies ran while one was open for 1% of the time, Pallas kernels for 59%

profile of v1, /device:TPU:0, one launch (start us, length us, event | category | flops | bytes accessed | tf_op | source)
XLA Modules:
  0.0 389.0 jit_solution(7323889229386529568)
XLA Ops:
  6.5 1.9 fusion.44
  8.5 3.1 fusion.46
  11.6 0.0 reduce-scatter.3.cloned.1.call-start
  11.7 1.1 pad_maximum_fusion.1.refs_0_
  12.8 1.2 pad_maximum_fusion.refs_2_
  14.0 230.4 %shard_map.109 = (bf16[2048,2048]{1,0:T(8,128)(2,1)}, bf16[1024,2048]{1,0:T(8,128)(2,1)}, bf16[2048,2816]{1,0:T(8,128)(2,1)}, bf16[1408,2048]{1,0:T(8,128)(2,1)}) custom-call(bf16[256,2048]{1,0:T(8,128)(2,1)} %pad_maximum_fusion.1.refs_0_, bf16[1024,256]{1,0:T(8,128)(2,1)} %refs_1_.1, bf16[256,2816]{1,0:T(8,128)(2,1)} %pad_maximum_fusion.refs_2_, ...), custom_call_target="tpu_custom_call" | custom-call | tf_op jit(solution)/shard_map/pallas_call | solution.py:196
  244.4 0.1 fusion.61
  244.6 2.3 fusion.58
  246.9 10.0 %convolution_convert_fusion = bf16[768,2048]{1,0:T(8,128)(2,1)S(1)} fusion(bf16[768,2048]{1,0:T(8,128)(2,1)} %all-gather.3.cloned.1.call-done, bf16[2048,2048]{1,0:T(8,128)(2,1)} %get-tuple-element.62), kind=kOutput, calls=%fused_computation.51 | convolution fusion | flops 6444023808 | bytes 14680064 | tf_op jit(solution)/shard_map/dot_general | solution.py:323
  256.9 2.5 slice_convert_fusion
  259.4 0.3 copy-done.3
  259.6 3.2 reshape.150
  262.8 3.1 reshape.152
  265.9 2.3 reshape_reshape.3
  268.2 1.8 copy.58
  270.1 0.5 copy-done.5
  270.6 1.1 fusion.63
  271.7 0.4 subtract_convert_fusion
  272.1 1.0 maximum_bitcast_fusion
  273.1 1.0 fusion.56
  274.1 28.8 %while.15 = (s32[]{:T(128)}, f32[2,256,512]{2,1,0:T(8,128)S(1)}, f32[6,2,128,512]{3,2,1,0:T(8,128)}, bf16[6,2,128,256]{3,2,0,1:T(8,128)(2,1)}, bf16[6,2,128,512]...) while((s32[]{:T(128)}, f32[2,256,512]{2,1,0:T(8,128)S(1)}, ...), condition=%wide.region_2.4_spmd.clone.clone.clone, body=%wide.region_1.3_spmd.clone.clone.clone.sunk | while | flops 186188304 | bytes 5858980 | solution.py:291
  274.1 0.1 multiply_exponential_fusion.6
  274.2 1.1 convolution_multiply_fusion.3
  275.3 2.1 fusion.83
  277.5 1.4 convolution_add_fusion.3
  278.9 0.1 multiply_exponential_fusion.6
  279.0 1.1 convolution_multiply_fusion.3
  280.1 2.1 fusion.83
  282.3 1.4 convolution_add_fusion.3
  283.7 0.1 multiply_exponential_fusion.6
  283.8 1.1 convolution_multiply_fusion.3
  284.9 2.1 fusion.83
  287.1 1.4 convolution_add_fusion.3
  288.5 0.1 multiply_exponential_fusion.6
  288.6 1.1 convolution_multiply_fusion.3
  289.7 2.1 fusion.83
  291.9 1.4 convolution_add_fusion.3
  293.3 0.1 multiply_exponential_fusion.6
  293.4 1.1 convolution_multiply_fusion.3
  294.5 2.1 fusion.83
  296.7 1.4 convolution_add_fusion.3
  298.1 0.1 multiply_exponential_fusion.6
  298.2 1.1 convolution_multiply_fusion.3
  299.3 2.1 fusion.83
  301.5 1.4 convolution_add_fusion.3
  302.9 2.2 multiply_reduce_fusion
  305.1 0.2 copy.39
  305.3 1.3 mul.286
  306.6 0.8 copy.48
  307.3 1.1 copy-done.2
  308.5 2.4 copy.38
  310.9 0.8 copy.47
  311.7 1.4 copy-done.14
  313.1 4.8 %convolution_convert_fusion.1 = bf16[768,2048]{1,0:T(8,128)(2,1)} fusion(bf16[1024,2048]{1,0:T(8,128)(2,1)S(1)} %copy-done.14, f32[768,1024]{1,0:T(8,128)S(1)} %bitcast.73, f32[768,1024]{1,0:T(8,128)S(1)} %bitcast.72, f32[1024]{0:T(1024)S(1)} %copy-done.15), kind=kOutput, calls=%fused_computation.52 | convolution fusion | flops 3225157632 | bytes 13635584 | tf_op jit(solution)/shard_map/dot_general | solution.py:342
  317.9 0.0 all-gather.5.cloned.1.call-start
  318.0 8.1 %reduce-scatter.3.cloned.1.call-done = bf16[384,2048]{1,0:T(8,128)(2,1)} async-done(((bf16[768,2048]{1,0:T(8,128)(2,1)}), bf16[384,2048]{1,0:T(8,128)(2,1)}) %reduce-scatter.3.cloned.1.call-update) | async-done | bytes 1572880 | tf_op jit(solution)/shard_map/reduce_scatter | solution.py:341
  326.1 2.1 fusion.48
  328.2 1.9 fusion.50
  330.1 0.0 reduce-scatter.5.cloned.1.call-start
  330.2 13.5 %all-gather.5.cloned.1.call-done = bf16[768,2048]{1,0:T(8,128)(2,1)} async-done(((bf16[384,2048]{1,0:T(8,128)(2,1)}), bf16[768,2048]{1,0:T(8,128)(2,1)}) %all-gather.5.cloned.1.call-update) | async-done | bytes 3145744 | tf_op jit(solution)/shard_map/all_gather | solution.py:351
  343.7 13.7 %fusion.65 = f32[768,2816]{1,0:T(8,128)S(1)} fusion(bf16[768,2048]{1,0:T(8,128)(2,1)} %all-gather.5.cloned.1.call-done, bf16[2048,2816]{1,0:T(8,128)(2,1)} %get-tuple-element.65), kind=kOutput, calls=%fused_computation.97 | convolution fusion | flops 8858370048 | bytes 23330816 | tf_op jit(solution)/shard_map/dot_general | solution.py:350
  357.4 9.2 %convolution_convert_fusion.2 = bf16[768,2048]{1,0:T(8,128)(2,1)} fusion(bf16[1408,2048]{1,0:T(8,128)(2,1)} %get-tuple-element.66, f32[768,2816]{1,0:T(8,128)S(1)} %fusion.65), kind=kOutput, calls=%fused_computation.53 | convolution fusion | flops 4437245952 | bytes 17563648 | tf_op jit(solution)/shard_map/dot_general | solution.py:358
  366.6 12.5 %reduce-scatter.5.cloned.1.call-done = bf16[384,2048]{1,0:T(8,128)(2,1)} async-done(((bf16[768,2048]{1,0:T(8,128)(2,1)}), bf16[384,2048]{1,0:T(8,128)(2,1)}) %reduce-scatter.5.cloned.1.call-update) | async-done | bytes 1572880 | tf_op jit(solution)/shard_map/reduce_scatter | solution.py:357
  379.1 3.4 fusion.51
  (52 shorter events, 0.4 us)
Async XLA Ops:
  6.5 5.1 %copy-start.12 = (bf16[256,512]{1,0:T(8,128)(2,1)S(1)}, bf16[256,512]{1,0:T(8,128)(2,1)}, u32[]{:S(2)}) copy-start(bf16[256,512]{1,0:T(8,128)(2,1)} %param.17) | copy-start | bytes 786436
  6.5 5.1 %copy-start.11 = (bf16[256,512]{1,0:T(8,128)(2,1)S(1)}, bf16[256,512]{1,0:T(8,128)(2,1)}, u32[]{:S(2)}) copy-start(bf16[256,512]{1,0:T(8,128)(2,1)} %param.18) | copy-start | bytes 786436
  6.5 5.1 %copy-start.10 = (bf16[256,1024]{1,0:T(8,128)(2,1)S(1)}, bf16[256,1024]{1,0:T(8,128)(2,1)}, u32[]{:S(2)}) copy-start(bf16[256,1024]{1,0:T(8,128)(2,1)} %param.19) | copy-start | bytes 1572868
  6.5 240.3 %all-gather.3.cloned.1.call-start = ((), (), s32[]{:S(2)}) async-start(), calls=%async_computation.2 | async-start | bytes 4718592 | tf_op jit(solution)/shard_map/all_gather | solution.py:324
  8.4 4.4 %copy-start.8 = (bf16[256,1408]{1,0:T(8,128)(2,1)S(1)}, bf16[256,1408]{1,0:T(8,128)(2,1)}, u32[]{:S(2)}) copy-start(bf16[256,1408]{1,0:T(8,128)(2,1)} %param.24) | copy-start | bytes 2162692
  8.4 4.3 %copy-start.9 = (bf16[256,1408]{1,0:T(8,128)(2,1)S(1)}, bf16[256,1408]{1,0:T(8,128)(2,1)}, u32[]{:S(2)}) copy-start(bf16[256,1408]{1,0:T(8,128)(2,1)} %param.23) | copy-start | bytes 2162692
  11.6 314.5 %reduce-scatter.3.cloned.1.call-start = ((), (), s32[]{:S(2)}) async-start(), calls=%async_computation.3 | async-start | bytes 4718592 | tf_op jit(solution)/shard_map/reduce_scatter | solution.py:341
  256.9 2.8 copy-start.3
  259.6 6.2 %slice-start = ((bf16[768,2048]{1,0:T(8,128)(2,1)}), bf16[768,1024]{1,0:T(8,128)(2,1)S(1)}, s32[]{:S(2)}) async-start(bf16[768,2048]{1,0:T(8,128)(2,1)} %copy-done.3), calls=%async_computation.6 | async-start | bytes 3145728 | tf_op jit(solution)/shard_map/slice | solution.py:334
  268.2 1.9 copy-start.4
  268.2 2.4 copy-start.5
  270.6 1.1 copy-start.6
  270.6 1.1 copy-start.7
  306.6 1.9 copy-start.2
  310.9 2.2 copy-start.14
  310.9 2.2 copy-start.15
  317.9 8.2 %copy-start = (bf16[384,2048]{1,0:T(8,128)(2,1)S(1)}, bf16[384,2048]{1,0:T(8,128)(2,1)}, u32[]{:S(2)}) copy-start(bf16[384,2048]{1,0:T(8,128)(2,1)} %param.15) | copy-start | bytes 4718596
  317.9 10.3 %copy-start.13 = (f32[2048]{0:T(1024)S(1)}, f32[2048]{0:T(1024)}, u32[]{:S(2)}) copy-start(f32[2048]{0:T(1024)} %param.22) | copy-start | bytes 24580
  317.9 25.8 %all-gather.5.cloned.1.call-start = ((), (), s32[]{:S(2)}) async-start(), calls=%async_computation.4 | async-start | bytes 4718592 | tf_op jit(solution)/shard_map/all_gather | solution.py:351
  326.1 2.1 copy-start.1
  330.1 48.9 %reduce-scatter.5.cloned.1.call-start = ((), (), s32[]{:S(2)}) async-start(), calls=%async_computation.5 | async-start | bytes 4718592 | tf_op jit(solution)/shard_map/reduce_scatter | solution.py:357
Sparse Core Ops, SparseCore 0:
  11.7 14.8 all-gather.2
  318.1 8.0 reduce-scatter.2
  330.3 13.4 all-gather.4
  366.7 12.3 reduce-scatter.4

commit v2 on v1

--- a/solution.py
+++ b/solution.py
@@ -148,11 +148,65 @@
             self.each(s, sent)
 
 
-def gather_kernel(depth, axes, *refs):
+def rotated(v, cosine, sine):
+    half = v.shape[-1] // 2
+    first, second = v[:, :half], v[:, half:]
+    return jnp.concatenate(
+        [first * cosine - second * sine, second * cosine + first * sine], axis=-1
+    )
+
+
+def column_dot(left, right, out, width=256):
+    @pl.loop(0, out.shape[1] // width)
+    def _(c):
+        cols = pl.ds(pl.multiple_of(c * width, width), width)
+        out[:, cols] = jnp.dot(
+            left[...], right[:, cols], preferred_element_type=jnp.float32
+        ).astype(out.dtype)
+
+
+def retain_head(h, heads, tables, proj, memory, head_out):
+    cos_ref, sin_ref, inside, query_decay, key_decay, block_decay, gain = tables
+    block = inside.shape[-1]
+    memory[...] = jnp.zeros_like(memory)
+    q_cols = pl.ds(h * DK, DK)
+    k_cols = pl.ds((heads + h) * DK, DK)
+    v_cols = pl.ds(2 * heads * DK + h * DV, DV)
+
+    @pl.loop(0, proj.shape[0] // block)
+    def _(b):
+        rows = pl.ds(pl.multiple_of(b * block, block), block)
+        cosine, sine = cos_ref[rows, :], sin_ref[rows, :]
+        q = rotated(proj[rows, q_cols].astype(jnp.float32), cosine, sine).astype(jnp.bfloat16)
+        k = rotated(proj[rows, k_cols].astype(jnp.float32), cosine, sine) * DK ** (-0.5)
+        k = k.astype(jnp.bfloat16)
+        v = proj[rows, v_cols]
+        scores = lax.dot_general(
+            q, k, (((1,), (1,)), ((), ())), preferred_element_type=jnp.float32
+        )
+        weights = (scores * inside[h]).astype(jnp.bfloat16)
+        state = memory[...]
+        kept = jnp.dot(weights, v, preferred_element_type=jnp.float32) + query_decay[h] * jnp.dot(
+            q, state.astype(jnp.bfloat16), preferred_element_type=jnp.float32
+        )
+        decayed = (k.astype(jnp.float32) * key_decay[h]).astype(jnp.bfloat16)
+        memory[...] = state * block_decay[h] + lax.dot_general(
+            decayed, v, (((0,), (0,)), ((), ())), preferred_element_type=jnp.float32
+        )
+        scale = lax.rsqrt(jnp.mean(kept * kept, axis=-1, keepdims=True) + norm_eps)
+        head_out[rows, pl.ds(h * DV, DV)] = (
+            kept * scale * gain[:, pl.ds(h * DV, DV)]
+        ).astype(jnp.bfloat16)
+
+
+def layer_kernel(depth, axes, *refs):
     count = len(axes)
-    shards, fulls = refs[:count], refs[count : 2 * count]
-    held = refs[2 * count : 3 * count]
-    send_sem, recv_sem, load_sem, store_sem = refs[3 * count :]
+    shards, refs = refs[:count], refs[count:]
+    x_ref, tables, refs = refs[0], refs[1:8], refs[8:]
+    fulls, part, refs = refs[:count], refs[count], refs[count + 1 :]
+    held, refs = refs[:count], refs[count:]
+    mixer, out_w, proj, memory, head_out, send_sem, recv_sem, load_sem, store_sem, fetch_sem = refs
+    heads = tables[2].shape[0]
     ex = Exchange(depth, shards, fulls, axes, send_sem, recv_sem)
     loads = [pltpu.make_async_copy(shards[w], held[w], load_sem.at[w]) for w in range(count)]
     for copy in loads:
@@ -160,12 +214,13 @@
     ex.barrier()
     fs = lax.axis_index("fs")
     stores = [
-        pltpu.make_async_copy(
-            held[w], ex.slot(w, fs, 0, shards[w].shape[0]), store_sem.at[w]
-        )
+        pltpu.make_async_copy(held[w], ex.slot(w, fs, 0, shards[w].shape[0]), store_sem.at[w])
         for w in range(count)
     ]
+    fetch_mixer = pltpu.make_async_copy(fulls[0], mixer, fetch_sem.at[0])
+    fetch_out = pltpu.make_async_copy(fulls[1], out_w, fetch_sem.at[1])
     pace = depth - 1
+    ready = depth + 1
     for tick in range(pace * (count - 1) + depth + 2):
         for w in range(count):
             t = tick - pace * w
@@ -175,17 +230,33 @@
             for load, store in zip(loads, stores):
                 load.wait()
                 store.start()
-    for copy in stores:
-        copy.wait()
+        if tick == 1:
+            for copy in stores:
+                copy.wait()
+        if tick == ready:
+            fetch_mixer.start()
+        if tick == ready + 1:
+            fetch_mixer.wait()
+            column_dot(x_ref, mixer, proj)
+        for h in range(heads):
+            if tick == ready + 2 + h // (heads // 2 if heads > 1 else 1):
+                retain_head(h, heads, tables, proj, memory, head_out)
+        if tick == pace + ready:
+            fetch_out.start()
+        if tick == pace + ready + 1:
+            fetch_out.wait()
+            column_dot(head_out, out_w, part)
     for w in range(count):
         ex.drain(w)
 
 
-def gather_all(shards, axes):
+def fits(shards):
+    whole = all(s.shape[0] % (UNITS * 16) == 0 and s.shape[1] % 128 == 0 for s in shards)
+    return whole and lax.axis_size("rep") == 2 and lax.axis_size("fs") == 8
+
+
+def layer_start(shards, axes, normed, tables):
     size = lax.axis_size("fs")
-    fits = all(s.shape[0] % (UNITS * 16) == 0 and s.shape[1] % 128 == 0 for s in shards)
-    if lax.axis_size("rep") != 2 or size % 2 or not fits:
-        return [lax.all_gather(s, "fs", axis=a, tiled=True) for s, a in zip(shards, axes)]
     depth = size // 2
     count = len(shards)
     shapes = []
@@ -193,20 +264,31 @@
         shape = list(s.shape)
         shape[a] *= size
         shapes.append(jax.ShapeDtypeStruct(tuple(shape), s.dtype))
+    rows = normed.shape[0]
+    values = shapes[1].shape[0]
+    part = jax.ShapeDtypeStruct((rows, shapes[1].shape[1]), jnp.bfloat16)
+    near = pl.BlockSpec(memory_space=pltpu.VMEM)
+    far = pl.BlockSpec(memory_space=pl.ANY)
     return pl.pallas_call(
-        functools.partial(gather_kernel, depth, tuple(axes)),
-        out_shape=shapes,
-        in_specs=[pl.BlockSpec(memory_space=pl.ANY)] * count,
-        out_specs=[pl.BlockSpec(memory_space=pl.ANY)] * count,
+        functools.partial(layer_kernel, depth, tuple(axes)),
+        out_shape=shapes + [part],
+        in_specs=[far] * count + [near] * (1 + len(tables)),
+        out_specs=[far] * count + [near],
         scratch_shapes=[pltpu.VMEM(s.shape, s.dtype) for s in shards]
         + [
+            pltpu.VMEM(shapes[0].shape, jnp.bfloat16),
+            pltpu.VMEM(shapes[1].shape, jnp.bfloat16),
+            pltpu.VMEM((rows, shapes[0].shape[1]), jnp.bfloat16),
+            pltpu.VMEM((DK, DV), jnp.float32),
+            pltpu.VMEM((rows, values), jnp.bfloat16),
             pltpu.SemaphoreType.DMA((count, 5, depth)),
             pltpu.SemaphoreType.DMA((count, 4, depth)),
             pltpu.SemaphoreType.DMA((count,)),
             pltpu.SemaphoreType.DMA((count,)),
+            pltpu.SemaphoreType.DMA((2,)),
         ],
         compiler_params=pltpu.CompilerParams(collective_id=0, has_side_effects=True),
-    )(*shards)
+    )(*shards, normed, *tables)
 
 
 DK = 256
@@ -224,14 +306,18 @@
     return (scaled * gain).astype(jnp.bfloat16)
 
 
+def rotation(length_total, half_width):
+    position = jnp.arange(length_total, dtype=jnp.float32)
+    inverse = 1.0 / rope_base ** jnp.linspace(0.0, 1.0, half_width, dtype=jnp.float32)
+    angle = position[:, None] * inverse[None, :]
+    return (jnp.cos(angle), jnp.sin(angle))
+
+
 def rotate(vectors):
     length_total = vectors.shape[0]
     half_width = vectors.shape[-1] // 2
-    position = jnp.arange(length_total, dtype=jnp.float32)
-    inverse = 1.0 / rope_base ** jnp.linspace(0.0, 1.0, half_width, dtype=jnp.float32)
-    angle = position[:, None] * inverse[None, :]
-    cosine = jnp.cos(angle)[:, None, :]
-    sine = jnp.sin(angle)[:, None, :]
+    cosine, sine = rotation(length_total, half_width)
+    cosine, sine = cosine[:, None, :], sine[:, None, :]
     first = vectors[..., :half_width]
     second = vectors[..., half_width:]
     return jnp.concatenate(
@@ -317,33 +403,36 @@
     normed = rms_scale(resid, mix_gain)
     mixer_shard = jnp.concatenate([query_weight, key_weight, value_weight], axis=1)
     mlp_shard = jnp.concatenate([gate_weight, up_weight], axis=1)
-    mixer_full, out_full, mlp_full, down_full = gather_all(
-        [mixer_shard, out_weight, mlp_shard, down_weight], [0, 1, 0, 1]
-    )
-    projected = jnp.dot(
-        lax.all_gather(normed, "tp", axis=0, tiled=True),
-        mixer_full,
-        preferred_element_type=jnp.float32,
-    ).astype(jnp.bfloat16)
-    queries = projected[:, :key_cols].astype(jnp.float32).reshape(length_total, heads_here, DK)
-    keys = (
-        projected[:, key_cols : 2 * key_cols]
-        .astype(jnp.float32)
-        .reshape(length_total, heads_here, DK)
-    )
-    values = projected[:, 2 * key_cols :].reshape(length_total, heads_here, DV)
-    query_rot = rotate(queries).astype(jnp.bfloat16)
-    key_rot = (rotate(keys) * DK ** (-0.5)).astype(jnp.bfloat16)
+    normed_full = lax.all_gather(normed, "tp", axis=0, tiled=True)
     head_ids = lax.axis_index("tp") * heads_here + jnp.arange(heads_here, dtype=jnp.int32)
-    retained = retain(query_rot, key_rot, values, head_ids, BLOCK)
-    head_out = head_scale(retained, head_gain)
-    selected = head_out
-    mixer_sum = lax.psum_scatter(
-        jnp.dot(selected, out_full, preferred_element_type=jnp.float32).astype(jnp.bfloat16),
-        "tp",
-        scatter_dimension=0,
-        tiled=True,
-    ).astype(jnp.float32)
+    pieces = [mixer_shard, out_weight, mlp_shard, down_weight]
+    if fits(pieces) and length_total % BLOCK == 0:
+        inside, query_decay, key_decay, block_decay = decay_tables(head_ids, BLOCK)
+        tables = [
+            *rotation(length_total, DK // 2),
+            inside,
+            query_decay[:, :, None],
+            key_decay[:, :, None],
+            jnp.broadcast_to(block_decay[:, None, None], (heads_here, DK, 1)),
+            head_gain[None, :],
+        ]
+        _, _, mlp_full, down_full, part = layer_start(pieces, [0, 1, 0, 1], normed_full, tables)
+    else:
+        mixer_full, out_full, mlp_full, down_full = (
+            lax.all_gather(s, "fs", axis=a, tiled=True) for s, a in zip(pieces, [0, 1, 0, 1])
+        )
+        projected = jnp.dot(
+            normed_full, mixer_full, preferred_element_type=jnp.float32
+        ).astype(jnp.bfloat16)
+        both_keys = projected[:, : 2 * key_cols].astype(jnp.float32)
+        both_keys = both_keys.reshape(length_total, 2, heads_here, DK)
+        values = projected[:, 2 * key_cols :].reshape(length_total, heads_here, DV)
+        query_rot = rotate(both_keys[:, 0]).astype(jnp.bfloat16)
+        key_rot = (rotate(both_keys[:, 1]) * DK ** (-0.5)).astype(jnp.bfloat16)
+        retained = retain(query_rot, key_rot, values, head_ids, BLOCK)
+        head_out = head_scale(retained, head_gain)
+        part = jnp.dot(head_out, out_full, preferred_element_type=jnp.float32).astype(jnp.bfloat16)
+    mixer_sum = lax.psum_scatter(part, "tp", scatter_dimension=0, tiled=True).astype(jnp.float32)
     middle = (resid.astype(jnp.float32) + mixer_sum).astype(jnp.bfloat16)
     normed_mlp = rms_scale(middle, mlp_gain)
     local_units = gate_weight.shape[1]

time: 390 us -> 335 us (0.86)
  matrix products: 65.7 us -> 22.8 us
  local copies, waits for them, and re-layouts: 20.2 us -> 0.83 us
  waiting for transfers between devices: 34.2 us -> 44 us
  other arithmetic: 24.8 us -> 18.5 us
  Pallas kernels: 230 us -> 235 us
    dot_general x20 -> x0, matrix products: 42.9 us -> none  [the longest x6 12.8 us: advance(): jnp.einsum('hlm,hmv->hlv', weights, value_block, preferred_element_type=j...]
    all_gather x1, waiting for transfers between devices: 0.01 us -> 8.61 us  [shards(): normed_full = lax.all_gather(normed, 'tp', axis=0, tiled=True)]
    reshape x2 -> x0, local copies, waits for them, and re-layouts: 6.22 us -> none  [the longest x1 3.17 us: shards(): keys = projected[:, key_cols:2 * key_cols].astype(jnp.float32).reshape(le...]
    unnamed x34 -> x16, local copies, waits for them, and re-layouts: 4.87 us -> 0.04 us
    pallas_call x1, Pallas kernels: 230 us -> 235 us  [layer_start(): pl.pallas_call(functools.partial(layer_kernel, depth, tuple(axes)), out_s...]
    another operation x2 -> x0, local copies, waits for them, and re-layouts: 4.18 us -> none  [blocks(): tensor.reshape(count, block, heads, tensor.shape[-1]).transpose(0, 2, 1, 3)]
  transfers between devices with their start and end apart: 4 -> 4, of which waited for: 3 -> 4; matrix products, arithmetic and copies ran while one was open for 1% -> 2% of each run, Pallas kernels for 59% -> 0%
where the time goes in v2:
time: 335 us
  Pallas kernels  235 us (70%)
  waiting for transfers between devices  44 us (13%)
  matrix products  22.8 us (7%)
  other arithmetic  18.5 us (6%)
  between operations  13.2 us (4%)
    pallas_call x1, Pallas kernels, layer_start(): pl.pallas_call(functools.partial(layer_kernel, depth, tuple(axes)), out_s...  235 us
    dot_general x1, matrix products, shards(): jnp.dot(lax.all_gather(normed_mlp, 'tp', axis=0, tiled=True), mlp_full, p...  13.7 us
    all_gather x1, waiting for transfers between devices, shards(): lax.all_gather(normed_mlp, 'tp', axis=0, tiled=True)  13.3 us
    reduce_scatter x1, waiting for transfers between devices, shards(): lax.psum_scatter(jnp.dot(selected, down_full, preferred_element_type=jnp....  12.5 us
    reduce_scatter x1, waiting for transfers between devices, shards(): lax.psum_scatter(part, 'tp', scatter_dimension=0, tiled=True)  9.44 us
    dot_general x1, matrix products, shards(): jnp.dot(selected, down_full, preferred_element_type=jnp.float32)  9.17 us
    all_gather x1, waiting for transfers between devices, shards(): normed_full = lax.all_gather(normed, 'tp', axis=0, tiled=True)  8.61 us
  transfers between devices with their start and end apart: 4, of which 4 were waited for; matrix products, arithmetic and copies ran while one was open for 2% of the time, Pallas kernels for 0%

profile of v2, /device:TPU:0, one launch (start us, length us, event | category | flops | bytes accessed | tf_op | source)
XLA Modules:
  0.0 334.6 jit_solution(11084346809004908251)
XLA Ops:
  6.5 0.0 all-gather.3.cloned.1.call-start
  6.5 1.8 fusion.1
  8.3 0.0 copy-start.4
  8.3 0.0 copy-start.5
  8.3 0.0 copy-start.6
  8.4 3.1 fusion.3
  11.4 0.0 copy-start.2
  11.4 0.0 copy-start.3
  11.4 0.0 all-gather.3.cloned.1.call-update
  11.5 0.0 reduce-scatter.3.cloned.1.call-start
  11.5 0.1 fusion.15
  11.7 0.7 exponential_select_fusion.refs_7_
  12.5 0.8 multiply_exponential_fusion
  13.3 2.2 fusion.11
  15.5 0.0 copy-done.4
  15.5 0.0 copy-done.5
  15.5 0.0 copy-done.6
  15.5 1.1 pad_maximum_fusion.1.refs_0_
  16.6 0.0 copy-done.2
  16.6 0.0 copy-done.3
  16.6 1.2 pad_maximum_fusion.refs_2_
  17.9 8.6 %all-gather.3.cloned.1.call-done.refs_4_ = bf16[768,2048]{1,0:T(8,128)(2,1)} async-done(((bf16[384,2048]{1,0:T(8,128)(2,1)}), bf16[768,2048]{1,0:T(8,128)(2,1)}) %all-gather.3.cloned.1.call-update) | async-done | bytes 3145744 | tf_op jit(solution)/shard_map/all_gather | solution.py:406
  26.5 0.8 broadcast_in_dim.16.refs_10_
  27.2 234.9 %shard_map.109 = (bf16[2048,2048]{1,0:T(8,128)(2,1)}, bf16[1024,2048]{1,0:T(8,128)(2,1)}, bf16[2048,2816]{1,0:T(8,128)(2,1)}, bf16[1408,2048]{1,0:T(8,128)(2,1)}, bf16[768,2048]{1,0:T(8,128)(2,1)}) custom-call(bf16[256,2048]{1,0:T(8,128)(2,1)} %pad_maximum_fusion.1.refs_0_, bf16[1024,256]{1,0:T(8,128)(2,1)} %refs_1_.1, ...), custom_call_target="tpu_custom_call" | custom-call | tf_op jit(solution)/shard_map/pallas_call | solution.py:272
  262.2 0.0 copy-start
  262.2 0.0 copy-start.7
  262.2 0.0 reduce-scatter.3.cloned.1.call-update
  262.2 0.0 all-gather.5.cloned.1.call-start
  262.3 9.4 %reduce-scatter.3.cloned.1.call-done = bf16[384,2048]{1,0:T(8,128)(2,1)} async-done(((bf16[768,2048]{1,0:T(8,128)(2,1)}), bf16[384,2048]{1,0:T(8,128)(2,1)}) %reduce-scatter.3.cloned.1.call-update) | async-done | bytes 1572880 | tf_op jit(solution)/shard_map/reduce_scatter | solution.py:435
  271.7 0.0 copy-done
  271.7 0.0 copy-start.1
  271.7 2.1 fusion.5
  273.8 0.0 copy-done.7
  273.8 0.0 copy-done.1
  273.9 1.9 fusion.7
  275.7 0.0 all-gather.5.cloned.1.call-update
  275.8 0.2 reduce-scatter.5.cloned.1.call-start
  276.0 13.3 %all-gather.5.cloned.1.call-done = bf16[768,2048]{1,0:T(8,128)(2,1)} async-done(((bf16[384,2048]{1,0:T(8,128)(2,1)}), bf16[768,2048]{1,0:T(8,128)(2,1)}) %all-gather.5.cloned.1.call-update) | async-done | bytes 3145744 | tf_op jit(solution)/shard_map/all_gather | solution.py:440
  289.3 13.7 %fusion.17 = f32[768,2816]{1,0:T(8,128)S(1)} fusion(bf16[768,2048]{1,0:T(8,128)(2,1)} %all-gather.5.cloned.1.call-done, bf16[2048,2816]{1,0:T(8,128)(2,1)} %get-tuple-element.9), kind=kOutput, calls=%fused_computation.39 | convolution fusion | flops 8858370048 | bytes 23330816 | tf_op jit(solution)/shard_map/dot_general | solution.py:439
  303.0 9.2 %convolution_convert_fusion = bf16[768,2048]{1,0:T(8,128)(2,1)} fusion(bf16[1408,2048]{1,0:T(8,128)(2,1)} %get-tuple-element.10, f32[768,2816]{1,0:T(8,128)S(1)} %fusion.17), kind=kOutput, calls=%fused_computation.8 | convolution fusion | flops 4437245952 | bytes 17563648 | tf_op jit(solution)/shard_map/dot_general | solution.py:447
  312.2 0.0 reduce-scatter.5.cloned.1.call-update
  312.2 12.5 %reduce-scatter.5.cloned.1.call-done = bf16[384,2048]{1,0:T(8,128)(2,1)} async-done(((bf16[768,2048]{1,0:T(8,128)(2,1)}), bf16[384,2048]{1,0:T(8,128)(2,1)}) %reduce-scatter.5.cloned.1.call-update) | async-done | bytes 1572880 | tf_op jit(solution)/shard_map/reduce_scatter | solution.py:446
  324.7 3.4 %fusion.8 = bf16[384,2048]{1,0:T(8,128)(2,1)} fusion(bf16[384,2048]{1,0:T(8,128)(2,1)} %reduce-scatter.5.cloned.1.call-done, bf16[384,2048]{1,0:T(8,128)(2,1)S(1)} %copy-done.1, bf16[384,2048]{1,0:T(8,128)(2,1)S(1)} %copy-done), kind=kLoop, calls=%fused_computation.16 | loop fusion | flops 6291456 | bytes 6291456 | tf_op jit(solution)/shard_map/convert_element_type | solution.py:452
  (7 shorter events, 0.1 us)
Async XLA Ops:
  6.5 19.9 %all-gather.3.cloned.1.call-start = ((), (), s32[]{:S(2)}) async-start(), calls=%async_computation.2 | async-start | bytes 4718592 | tf_op jit(solution)/shard_map/all_gather | solution.py:406
  8.3 7.2 %copy-start.4 = (bf16[256,1024]{1,0:T(8,128)(2,1)S(1)}, bf16[256,1024]{1,0:T(8,128)(2,1)}, u32[]{:S(2)}) copy-start(bf16[256,1024]{1,0:T(8,128)(2,1)} %param.15) | copy-start | bytes 1572868
  8.3 7.2 %copy-start.5 = (bf16[256,512]{1,0:T(8,128)(2,1)S(1)}, bf16[256,512]{1,0:T(8,128)(2,1)}, u32[]{:S(2)}) copy-start(bf16[256,512]{1,0:T(8,128)(2,1)} %param.14) | copy-start | bytes 786436
  8.3 7.2 %copy-start.6 = (bf16[256,512]{1,0:T(8,128)(2,1)S(1)}, bf16[256,512]{1,0:T(8,128)(2,1)}, u32[]{:S(2)}) copy-start(bf16[256,512]{1,0:T(8,128)(2,1)} %param.13) | copy-start | bytes 786436
  11.4 5.2 %copy-start.2 = (bf16[256,1408]{1,0:T(8,128)(2,1)S(1)}, bf16[256,1408]{1,0:T(8,128)(2,1)}, u32[]{:S(2)}) copy-start(bf16[256,1408]{1,0:T(8,128)(2,1)} %param.20) | copy-start | bytes 2162692
  11.4 5.2 %copy-start.3 = (bf16[256,1408]{1,0:T(8,128)(2,1)S(1)}, bf16[256,1408]{1,0:T(8,128)(2,1)}, u32[]{:S(2)}) copy-start(bf16[256,1408]{1,0:T(8,128)(2,1)} %param.19) | copy-start | bytes 2162692
  11.5 260.3 %reduce-scatter.3.cloned.1.call-start = ((), (), s32[]{:S(2)}) async-start(), calls=%async_computation.3 | async-start | bytes 4718592 | tf_op jit(solution)/shard_map/reduce_scatter | solution.py:435
  262.2 9.5 %copy-start = (bf16[384,2048]{1,0:T(8,128)(2,1)S(1)}, bf16[384,2048]{1,0:T(8,128)(2,1)}, u32[]{:S(2)}) copy-start(bf16[384,2048]{1,0:T(8,128)(2,1)} %param.11) | copy-start | bytes 4718596
  262.2 11.7 %copy-start.7 = (f32[2048]{0:T(1024)S(1)}, f32[2048]{0:T(1024)}, u32[]{:S(2)}) copy-start(f32[2048]{0:T(1024)} %param.18) | copy-start | bytes 24580
  262.2 27.1 %all-gather.5.cloned.1.call-start = ((), (), s32[]{:S(2)}) async-start(), calls=%async_computation.4 | async-start | bytes 4718592 | tf_op jit(solution)/shard_map/all_gather | solution.py:440
  271.7 2.1 copy-start.1
  275.8 49.0 %reduce-scatter.5.cloned.1.call-start = ((), (), s32[]{:S(2)}) async-start(), calls=%async_computation.5 | async-start | bytes 4718592 | tf_op jit(solution)/shard_map/reduce_scatter | solution.py:446
Sparse Core Ops, SparseCore 0:
  11.6 14.8 all-gather.2
  262.3 9.3 reduce-scatter.2
  275.9 13.4 all-gather.4
  312.3 12.3 reduce-scatter.4

commit v3 on v2

--- a/solution.py
+++ b/solution.py
@@ -383,6 +383,29 @@
     return (scaled.reshape(retained.shape[0], -1) * gain).astype(jnp.bfloat16)
 
 
+def swap(rows):
+    return lax.ppermute(rows, "tp", [(0, 1), (1, 0)])
+
+
+def join_rows(rows):
+    if lax.axis_size("tp") != 2:
+        return lax.all_gather(rows, "tp", axis=0, tiled=True)
+    first = lax.axis_index("tp") == 0
+    got = swap(rows)
+    return jnp.concatenate([jnp.where(first, rows, got), jnp.where(first, got, rows)], axis=0)
+
+
+def share_sum(part):
+    if lax.axis_size("tp") != 2:
+        summed = lax.psum_scatter(part, "tp", scatter_dimension=0, tiled=True)
+        return summed.astype(jnp.float32)
+    count = part.shape[0] // 2
+    me = lax.axis_index("tp")
+    mine = lax.dynamic_slice_in_dim(part, me * count, count, axis=0)
+    theirs = lax.dynamic_slice_in_dim(part, (1 - me) * count, count, axis=0)
+    return mine.astype(jnp.float32) + swap(theirs).astype(jnp.float32)
+
+
 def shards(
     resid,
     mix_gain,
@@ -403,7 +426,7 @@
     normed = rms_scale(resid, mix_gain)
     mixer_shard = jnp.concatenate([query_weight, key_weight, value_weight], axis=1)
     mlp_shard = jnp.concatenate([gate_weight, up_weight], axis=1)
-    normed_full = lax.all_gather(normed, "tp", axis=0, tiled=True)
+    normed_full = join_rows(normed)
     head_ids = lax.axis_index("tp") * heads_here + jnp.arange(heads_here, dtype=jnp.int32)
     pieces = [mixer_shard, out_weight, mlp_shard, down_weight]
     if fits(pieces) and length_total % BLOCK == 0:
@@ -432,23 +455,20 @@
         retained = retain(query_rot, key_rot, values, head_ids, BLOCK)
         head_out = head_scale(retained, head_gain)
         part = jnp.dot(head_out, out_full, preferred_element_type=jnp.float32).astype(jnp.bfloat16)
-    mixer_sum = lax.psum_scatter(part, "tp", scatter_dimension=0, tiled=True).astype(jnp.float32)
+    mixer_sum = share_sum(part)
     middle = (resid.astype(jnp.float32) + mixer_sum).astype(jnp.bfloat16)
     normed_mlp = rms_scale(middle, mlp_gain)
     local_units = gate_weight.shape[1]
     both = jnp.dot(
-        lax.all_gather(normed_mlp, "tp", axis=0, tiled=True),
+        join_rows(normed_mlp),
         mlp_full,
         preferred_element_type=jnp.float32,
     )
     hidden_units = (jax.nn.silu(both[:, :local_units]) * both[:, local_units:]).astype(jnp.bfloat16)
     selected = hidden_units
-    mlp_sum = lax.psum_scatter(
-        jnp.dot(selected, down_full, preferred_element_type=jnp.float32).astype(jnp.bfloat16),
-        "tp",
-        scatter_dimension=0,
-        tiled=True,
-    ).astype(jnp.float32)
+    mlp_sum = share_sum(
+        jnp.dot(selected, down_full, preferred_element_type=jnp.float32).astype(jnp.bfloat16)
+    )
     return (middle.astype(jnp.float32) + mlp_sum).astype(jnp.bfloat16)
 
 

time: 335 us -> 296 us (0.88)
  waiting for transfers between devices: 44 us -> 10.1 us
  between operations: 13.2 us -> 0.13 us
  other arithmetic: 18.5 us -> 22.6 us
    all_gather x2 -> x0, waiting for transfers between devices: 22 us -> none  [the longest x1 13.3 us: shards(): lax.all_gather(normed_mlp, 'tp', axis=0, tiled=True)]
    reduce_scatter x2 -> x0, waiting for transfers between devices: 21.9 us -> none  [the longest x1 12.5 us: shards(): lax.psum_scatter(jnp.dot(selected, down_full, preferred_element_type=jnp....]
    ppermute x0 -> x4, waiting for transfers between devices: none -> 10.1 us  [swap(): return lax.ppermute(rows, 'tp', [(0, 1), (1, 0)])]
  transfers between devices with their start and end apart: 4 -> 4, of which waited for: 4 -> 3; matrix products, arithmetic and copies ran while one was open for 2% -> 3% of each run, Pallas kernels for 0% -> 0%
where the time goes in v3:
time: 296 us; the launch traced here: 295 us
  Pallas kernels  236 us (80%)
  other arithmetic  22.6 us (8%)
  matrix products  21.3 us (7%)
  waiting for transfers between devices  10.1 us (3%)
  local copies, waits for them, and re-layouts  3.73 us (1%)
    pallas_call x1, Pallas kernels, layer_start(): pl.pallas_call(functools.partial(layer_kernel, depth, tuple(axes)), out_s...  236 us
    dot_general x1, matrix products, shards(): jnp.dot(join_rows(normed_mlp), mlp_full, preferred_element_type=jnp.float32)  12.5 us
    ppermute x4, waiting for transfers between devices, swap(): return lax.ppermute(rows, 'tp', [(0, 1), (1, 0)])  10.1 us
    dot_general x1, matrix products, shards(): jnp.dot(selected, down_full, preferred_element_type=jnp.float32)  8.86 us
  transfers between devices with their start and end apart: 4, of which 3 were waited for; matrix products, arithmetic and copies ran while one was open for 3% of the time, Pallas kernels for 0%

profile of v3, /device:TPU:0, one launch (start us, length us, event | category | flops | bytes accessed | tf_op | source)
XLA Modules:
  0.0 295.3 jit_solution(8568732003343809043)
XLA Ops:
  0.0 0.0 copy-start.1
  0.0 1.8 fusion.1
  1.8 3.0 %fusion.3 = bf16[384,2048]{1,0:T(8,128)(2,1)} fusion(bf16[384,2048]{1,0:T(8,128)(2,1)} %param.11, f32[2048]{0:T(1024)} %param.12, f32[384]{0:T(512)S(1)} %add_rsqrt_fusion.1), kind=kLoop, calls=%fused_computation.11 | loop fusion | flops 3145728 | bytes 3155456 | tf_op jit(solution)/shard_map/convert_element_type | solution.py:306
  4.8 0.5 collective-permute-start
  5.4 0.1 fusion.19
  5.5 0.0 copy-start
  5.5 0.0 copy-start.2
  5.5 0.7 exponential_select_fusion.refs_7_
  6.3 0.8 multiply_exponential_fusion
  7.1 2.2 fusion.15
  9.3 0.0 copy-done.1
  9.3 2.2 pad_maximum_fusion.2.refs_0_
  11.6 2.6 pad_maximum_fusion.1.refs_2_
  14.1 0.0 collective-permute-done
  14.1 0.0 copy-done
  14.1 0.0 copy-done.2
  14.1 1.0 broadcast_select_fusion.3
  15.2 2.0 pad_maximum_fusion.refs_4_
  17.2 0.8 broadcast_in_dim.16.refs_10_
  18.0 236.4 %shard_map.109 = (bf16[2048,2048]{1,0:T(8,128)(2,1)}, bf16[1024,2048]{1,0:T(8,128)(2,1)}, bf16[2048,2816]{1,0:T(8,128)(2,1)}, bf16[1408,2048]{1,0:T(8,128)(2,1)}, bf16[768,2048]{1,0:T(8,128)(2,1)}) custom-call(bf16[256,2048]{1,0:T(8,128)(2,1)} %pad_maximum_fusion.2.refs_0_, bf16[1024,256]{1,0:T(8,128)(2,1)} %refs_1_.1, ...), custom_call_target="tpu_custom_call" | custom-call | tf_op jit(solution)/shard_map/pallas_call | solution.py:272
  254.4 2.7 constant_dynamic-slice_fusion.1
  257.1 0.0 collective-permute-start.1
  257.1 0.0 copy-start.3
  257.1 3.6 %collective-permute-done.1 = bf16[384,2048]{1,0:T(8,128)(2,1)S(1)} collective-permute-done((bf16[384,2048]{1,0:T(8,128)(2,1)}, bf16[384,2048]{1,0:T(8,128)(2,1)S(1)}, u32[]{:S(2)}, u32[]{:S(2)}) %collective-permute-start.1) | collective-permute-done | bytes 1572896 | tf_op jit(solution)/shard_map/ppermute | solution.py:387
  260.8 0.0 copy-start.4
  260.8 2.5 fusion.5
  263.3 0.0 copy-done.3
  263.3 0.4 fusion.7
  263.7 0.2 collective-permute-start.2
  263.9 3.3 %collective-permute-done.2 = bf16[384,2048]{1,0:T(8,128)(2,1)S(1)} collective-permute-done((bf16[384,2048]{1,0:T(8,128)(2,1)S(1)}, bf16[384,2048]{1,0:T(8,128)(2,1)S(1)}, u32[]{:S(2)}, u32[]{:S(2)}) %collective-permute-start.2) | collective-permute-done | bytes 1572896 | tf_op jit(solution)/shard_map/ppermute | solution.py:387
  267.2 0.0 slice-start
  267.2 1.1 broadcast_select_fusion.1
  268.3 0.0 copy-done.4
  268.3 0.0 slice-start.1
  268.3 12.5 %fusion.9 = f32[768,2816]{1,0:T(8,128)} fusion(bf16[2048,2816]{1,0:T(8,128)(2,1)S(1)} %copy-done.4, bf16[384,2048]{1,0:T(8,128)(2,1)S(1)} %get-tuple-element.14, bf16[384,2048]{1,0:T(8,128)(2,1)S(1)} %get-tuple-element.13), kind=kOutput, calls=%fused_computation.18 | convolution fusion | flops 8864661504 | bytes 23330816 | tf_op jit(solution)/shard_map/dot_general | solution.py:462
  280.7 0.0 slice-done
  280.8 0.0 slice-done.1
  280.8 8.9 %convolution_convert_fusion = bf16[768,2048]{1,0:T(8,128)(2,1)S(1)} fusion(bf16[1408,2048]{1,0:T(8,128)(2,1)S(1)} %bitcast.5, f32[768,2816]{1,0:T(8,128)} %fusion.9), kind=kOutput, calls=%fused_computation.8 | convolution fusion | flops 4437245952 | bytes 17563648 | tf_op jit(solution)/shard_map/dot_general | solution.py:470
  289.6 0.2 constant_dynamic-slice_fusion
  289.8 0.2 collective-permute-start.3
  290.0 3.2 %collective-permute-done.3 = bf16[384,2048]{1,0:T(8,128)(2,1)S(1)} collective-permute-done((bf16[384,2048]{1,0:T(8,128)(2,1)S(1)}, bf16[384,2048]{1,0:T(8,128)(2,1)S(1)}, u32[]{:S(2)}, u32[]{:S(2)}) %collective-permute-start.3) | collective-permute-done | bytes 1572896 | tf_op jit(solution)/shard_map/ppermute | solution.py:387
  293.3 2.0 fusion.8
  (8 shorter events, 0.1 us)
Async XLA Ops:
  0.0 9.3 %copy-start.1 = (bf16[256,512]{1,0:T(8,128)(2,1)S(1)}, bf16[256,512]{1,0:T(8,128)(2,1)}, u32[]{:S(2)}) copy-start(bf16[256,512]{1,0:T(8,128)(2,1)} %param.14) | copy-start | bytes 786436
  4.8 9.3 %collective-permute-start = (bf16[384,2048]{1,0:T(8,128)(2,1)}, bf16[384,2048]{1,0:T(8,128)(2,1)S(1)}, u32[]{:S(2)}, u32[]{:S(2)}) collective-permute-start(bf16[384,2048]{1,0:T(8,128)(2,1)} %fusion.3), channel_id=1, source_target_pairs={{0,1},{1,0},{2,3},{3,2},{4,5},{5,4},{6,7},{7,6},{8,9},{9,8},{10,11... | collective-permute-start | bytes 4718600 | tf_op jit(solution)/shard_map/ppermute | solution.py:387
  5.5 8.6 %copy-start = (bf16[384,2048]{1,0:T(8,128)(2,1)S(1)}, bf16[384,2048]{1,0:T(8,128)(2,1)}, u32[]{:S(2)}) copy-start(bf16[384,2048]{1,0:T(8,128)(2,1)} %param.11) | copy-start | bytes 4718596
  5.5 8.6 %copy-start.2 = (f32[2048]{0:T(1024)S(1)}, f32[2048]{0:T(1024)}, u32[]{:S(2)}) copy-start(f32[2048]{0:T(1024)} %param.12) | copy-start | bytes 24580
  257.1 3.6 %collective-permute-start.1 = (bf16[384,2048]{1,0:T(8,128)(2,1)}, bf16[384,2048]{1,0:T(8,128)(2,1)S(1)}, u32[]{:S(2)}, u32[]{:S(2)}) collective-permute-start(bf16[384,2048]{1,0:T(8,128)(2,1)} %constant_dynamic-slice_fusion.1), channel_id=1, source_target_pairs={{0,1},{1,0},{2,3},{3,2},{4,5},{5,4},{6,7},{7,6},{8,9},{9,8},{10,11... | collective-permute-start | bytes 4718600 | tf_op jit(solution)/shard_map/ppermute | solution.py:387
  257.1 6.1 %copy-start.3 = (f32[2048]{0:T(1024)S(1)}, f32[2048]{0:T(1024)}, u32[]{:S(2)}) copy-start(f32[2048]{0:T(1024)} %param.18) | copy-start | bytes 24580
  260.8 7.5 %copy-start.4 = (bf16[2048,2816]{1,0:T(8,128)(2,1)S(1)}, bf16[2048,2816]{1,0:T(8,128)(2,1)}, u32[]{:S(2)}) copy-start(bf16[2048,2816]{1,0:T(8,128)(2,1)} %get-tuple-element.9) | copy-start | bytes 34603012
  263.7 3.5 %collective-permute-start.2 = (bf16[384,2048]{1,0:T(8,128)(2,1)S(1)}, bf16[384,2048]{1,0:T(8,128)(2,1)S(1)}, u32[]{:S(2)}, u32[]{:S(2)}) collective-permute-start(bf16[384,2048]{1,0:T(8,128)(2,1)S(1)} %fusion.7), channel_id=1, source_target_pairs={{0,1},{1,0},{2,3},{3,2},{4,5},{5,4},{6,7},{7,6},{8,9},{9,8},{10,11... | collective-permute-start | bytes 4718600 | tf_op jit(solution)/shard_map/ppermute | solution.py:387
  267.2 13.6 %slice-start = ((s8[5767168]{0:T(1024)(128)(4,1)}), s8[4194304]{0:T(1024)(128)(4,1)S(1)}, s32[]{:S(2)}) async-start(s8[5767168]{0:T(1024)(128)(4,1)} %bitcast.4), calls=%async_computation | async-start | bytes 8388608
  268.3 12.5 %slice-start.1 = ((s8[5767168]{0:T(1024)(128)(4,1)}), s8[1572864]{0:T(1024)(128)(4,1)S(1)}, s32[]{:S(2)}) async-start(s8[5767168]{0:T(1024)(128)(4,1)} %bitcast.4), calls=%async_computation.1 | async-start | bytes 3145728
  289.8 3.5 %collective-permute-start.3 = (bf16[384,2048]{1,0:T(8,128)(2,1)S(1)}, bf16[384,2048]{1,0:T(8,128)(2,1)S(1)}, u32[]{:S(2)}, u32[]{:S(2)}) collective-permute-start(bf16[384,2048]{1,0:T(8,128)(2,1)S(1)} %constant_dynamic-slice_fusion), channel_id=1, source_target_pairs={{0,1},{1,0},{2,3},{3,2},{4,5},{5,4},{6,7},{7,6},{8,9},{9,8},{10,11... | collective-permute-start | bytes 4718600 | tf_op jit(solution)/shard_map/ppermute | solution.py:387
